TPU v7x, 32 devices: a whole 2x2x4 slice. The times are simulated.
32 devices in a mesh: sp: 16 (over z, y, x), tp: 2 (over core).
Axes of the slice: x: 2, y: 2, z: 4, core: 2. Of those that a mesh axis runs over, the one named last changes fastest.
Arguments:
- resid: bfloat16 [4096, 2048], P(('sp', 'tp')), may hold values from -6 to 6
- queries: bfloat16 [4096, 2048], P('sp', 'tp'), may hold values from -6 to 6
- keys: bfloat16 [4096, 1024], P('sp', 'tp'), may hold values from -6 to 6
- values: bfloat16 [4096, 1024], P('sp', 'tp'), may hold values from -6 to 6
- log_gates: float32 [16, 4096], P('tp'), as said below
- documents: int32 [4096], P('sp'), may hold values from 0 to 2, never falling along the last dimension, each value on 1 to 3072 neighbouring positions
- out_weight: bfloat16 [2048, 2048], P('tp'), may hold values from -0.125 to 0.125
- attn_gain: float32 [2048], replicated, may hold values from 0.1 to 1.9
- mlp_gain: float32 [2048], replicated, may hold values from 0.1 to 1.9
- gate_weight: bfloat16 [2048, 4096], P('sp', 'tp'), may hold values from -0.125 to 0.125
- up_weight: bfloat16 [2048, 4096], P('sp', 'tp'), may hold values from -0.125 to 0.125
- down_weight: bfloat16 [4096, 2048], P('tp', 'sp'), may hold values from -0.375 to 0.375
Outputs:
- mixed: bfloat16 [4096, 2048], P(('sp', 'tp'))
Inputs may be any that keep to these rules, and one draw needn't show every extreme that they name: `log_gates`: each head's row never rises from one position to the next and starts at or below 0. `documents`: document numbers never fall along the positions; one document spans exactly three quarters of the 4096 positions.
All inputs are finite; a program needn't handle non-finite values.
Results may differ from a plain program's by a relative error of at most 0.018.
Values may be sent and summed in bfloat16 or wider, within the bound.
A program may use at most 64 MiB of HBM per device.

v0:
```python
import math
import jax
import jax.numpy as jnp
from jax import lax
from jax.sharding import PartitionSpec as P

HD = 128


def local(
    resid,
    queries,
    keys,
    values,
    log_gates,
    documents,
    out_weight,
    attn_gain,
    mlp_gain,
    gate_weight,
    up_weight,
    down_weight,
):
    tok_rows = queries.shape[0]
    kv_dev = keys.shape[1] // HD
    heads_dev = log_gates.shape[0]
    group_size = heads_dev // kv_dev
    score_scale = 1.0 / math.sqrt(HD)
    own_start = lax.axis_index("sp") * tok_rows
    own_last = own_start + tok_rows - 1
    first_doc = documents[0]
    query_pos = own_start + lax.iota(jnp.int32, tok_rows)
    query_heads = queries.reshape(tok_rows, kv_dev, group_size, HD)
    key_gates_all = log_gates.reshape(kv_dev, group_size, log_gates.shape[1])
    query_gates = lax.dynamic_slice_in_dim(key_gates_all, own_start, tok_rows, 2)
    collected = (
        lax.all_gather(gate_weight, "sp", axis=0, tiled=True),
        lax.all_gather(up_weight, "sp", axis=0, tiled=True),
        lax.all_gather(down_weight, "sp", axis=1, tiled=True),
    )
    residual_rows = resid.astype(jnp.float32)

    def attend_block(running, key_rows, value_rows, doc_rows, first_row):
        run_max, run_sum, accumulated = running
        key_count = key_rows.shape[0]
        scores = (
            jnp.einsum(
                "tkgd,skd->kgts",
                query_heads,
                key_rows.reshape(key_count, kv_dev, HD),
                preferred_element_type=jnp.float32,
            )
            * score_scale
        )
        key_gates = lax.dynamic_slice_in_dim(key_gates_all, first_row, key_count, 2)
        scores = scores + query_gates[..., None] - key_gates[:, :, None, :]
        key_pos = first_row + lax.iota(jnp.int32, key_count)
        visible = (key_pos[None, :] <= query_pos[:, None]) & (
            doc_rows[None, :] == documents[:, None]
        )
        scores = jnp.where(visible, scores, jnp.float32(-1e30))
        new_max = jnp.maximum(run_max, jnp.max(scores, axis=-1))
        probs = jnp.where(visible, jnp.exp(scores - new_max[..., None]), jnp.float32(0.0))
        shrink = jnp.exp(run_max - new_max)
        run_sum = run_sum * shrink + jnp.sum(probs, axis=-1)
        weighted = jnp.einsum(
            "kgts,skd->kgtd",
            probs.astype(jnp.bfloat16),
            value_rows.reshape(key_count, kv_dev, HD),
            preferred_element_type=jnp.float32,
        )
        accumulated = accumulated * shrink[..., None] + weighted
        return (new_max, run_sum, accumulated)

    def maybe_attend(running, key_rows, value_rows, doc_rows, first_row):
        needed = (first_row <= own_last) & (doc_rows[-1] >= first_doc)

        def compute(state):
            return attend_block(state, key_rows, value_rows, doc_rows, first_row)

        def keep(state):
            return state

        return lax.cond(needed, compute, keep, running)

    start_state = (
        jnp.full((kv_dev, group_size, tok_rows), -1e30, jnp.float32),
        jnp.zeros((kv_dev, group_size, tok_rows), jnp.float32),
        jnp.zeros((kv_dev, group_size, tok_rows, HD), jnp.float32),
    )
    key_rows = lax.all_gather(keys, "sp", axis=0, tiled=True)
    value_rows = lax.all_gather(values, "sp", axis=0, tiled=True)
    doc_rows = lax.all_gather(documents, "sp", axis=0, tiled=True)
    key_count = key_rows.shape[0]
    block_len = math.gcd(key_count, 1024)

    def advance(block_index, inner):
        offset = block_index * block_len
        return maybe_attend(
            inner,
            lax.dynamic_slice_in_dim(key_rows, offset, block_len, 0),
            lax.dynamic_slice_in_dim(value_rows, offset, block_len, 0),
            lax.dynamic_slice_in_dim(doc_rows, offset, block_len, 0),
            offset,
        )

    run_max, run_sum, accumulated = lax.fori_loop(0, key_count // block_len, advance, start_state)
    attended = accumulated / run_sum[..., None]
    attended = (
        jnp.transpose(attended, (2, 0, 1, 3)).reshape(tok_rows, heads_dev * HD).astype(jnp.bfloat16)
    )
    rows_slice = attended
    projected = lax.psum_scatter(
        jnp.dot(rows_slice, out_weight, preferred_element_type=jnp.float32).astype(jnp.bfloat16),
        "tp",
        scatter_dimension=0,
        tiled=True,
    ).astype(jnp.float32)
    power = jnp.mean(projected * projected, axis=-1, keepdims=True)
    middle = residual_rows + attn_gain * projected * lax.rsqrt(power + 1e-06)
    middle_power = jnp.mean(middle * middle, axis=-1, keepdims=True)
    normed = (mlp_gain * middle * lax.rsqrt(middle_power + 1e-06)).astype(jnp.bfloat16)
    normed_all = lax.all_gather(normed, "tp", axis=0, tiled=True)
    gate_full, up_full, down_full = collected
    gate_act = jnp.dot(normed_all, gate_full, preferred_element_type=jnp.float32)
    up_act = jnp.dot(normed_all, up_full, preferred_element_type=jnp.float32)
    hidden = (jax.nn.silu(gate_act) * up_act).astype(jnp.bfloat16)
    rows_slice = hidden
    lowered = lax.psum_scatter(
        jnp.dot(rows_slice, down_full, preferred_element_type=jnp.float32).astype(jnp.bfloat16),
        "tp",
        scatter_dimension=0,
        tiled=True,
    ).astype(jnp.float32)
    return (middle + 0.5 * lowered).astype(jnp.bfloat16)


def solution(mesh):
    placed = (
        P(("sp", "tp"), None),
        P("sp", "tp"),
        P("sp", "tp"),
        P("sp", "tp"),
        P("tp", None),
        P("sp"),
        P("tp", None),
        P(),
        P(),
        P("sp", "tp"),
        P("sp", "tp"),
        P("tp", "sp"),
    )
    return jax.shard_map(
        local, mesh=mesh, in_specs=placed, out_specs=P(("sp", "tp"), None), check_vma=False
    )
```

profile of v0, /device:TPU:0, one launch (start us, length us, event | category | flops | bytes accessed | tf_op | source)
XLA Modules:
  0.0 661.0 jit_solution(3229841452047718858)
XLA Ops:
  6.5 1.8 copy.27
  8.4 1.8 copy.25
  11.3 1.2 copy.26
  14.0 43.0 %all-gather = s32[16,1,256]{2,1,0:T(1,128)S(1)} all-gather(s32[1,1,256]{2,1,0:T(1,128)} %bitcast.62), channel_id=1, replica_groups=mesh['sp'=16,'tp'=2] {'sp'}, dimensions={0}, use_global_device_ids=true | all-gather | bytes 17408 | tf_op jit(solution)/shard_map/all_gather | solution.py:93
  56.9 42.7 %all-gather.10.cloned.1.call-done = bf16[4096,512]{0,1:T(8,128)(2,1)} async-done(((bf16[256,512]{0,1:T(8,128)(2,1)}), bf16[4096,512]{0,1:T(8,128)(2,1)}) %all-gather.10.cloned.1.call-update) | async-done | bytes 4194320 | tf_op jit(solution)/shard_map/all_gather | solution.py:92
  99.7 87.7 %all-gather.8.cloned.1.call-done = bf16[4096,512]{0,1:T(8,128)(2,1)} async-done(((bf16[256,512]{0,1:T(8,128)(2,1)}), bf16[4096,512]{0,1:T(8,128)(2,1)}) %all-gather.8.cloned.1.call-update) | async-done | bytes 4194320 | tf_op jit(solution)/shard_map/all_gather | solution.py:91
  187.5 20.5 %while.18 = (s32[]{:T(128)}, f32[4,2,256]{2,1,0:T(2,128)S(1)}, f32[4,2,256]{2,1,0:T(2,128)S(1)}, f32[4,2,256,128]{3,2,1,0:T(8,128)S(1)}, s32[]{:T(128)}, /*index...) while((s32[]{:T(128)}, f32[4,2,256]{2,1,0:T(2,128)S(1)}, ...), condition=%wide.region_5.6_spmd.clone, body=%wide.region_0.5_spmd.clone.sunk | while | flops 1114903808 | bytes 35472848 | solution.py:107
  189.3 13.1 %conditional.3 = ((f32[4,2,256]{2,1,0:T(2,128)S(1)}, f32[4,2,256]{2,1,0:T(2,128)S(1)}, f32[4,2,256,128]{3,2,1,0:T(8,128)S(1)})) conditional(s32[]{:T(128)} %convert_element_type.92, (f32[4,2,256]{2,1,0:T(2,128)S(1)}, f32[4,2,256]{2,1,0:T(2,128)S(1)}, f32[4,2,256,128]{3,2,1,0:T(8,128)S(1)}) %tuple.52, (s32[]{:T(128)}, s32[]{:T(128)}, ...), branch_computations={%region_1.0_spmd, %region_2.4_spmd} | conditional | flops 1114903808 | bytes 35463248 | solution.py:84
  190.4 1.7 constant_dynamic-slice_fusion
  192.2 3.0 fusion.6
  195.2 3.0 fusion.5
  198.3 4.1 fusion.10
  208.5 4.4 convolution_convert_fusion
  213.0 32.8 %reduce-scatter.3.cloned.1.call-done = bf16[128,2048]{1,0:T(8,128)(2,1)} async-done(((bf16[256,2048]{1,0:T(8,128)(2,1)}), bf16[128,2048]{1,0:T(8,128)(2,1)}) %reduce-scatter.3.cloned.1.call-update) | async-done | bytes 524304 | tf_op jit(solution)/shard_map/reduce_scatter | solution.py:113
  247.1 1.4 multiply_reduce_fusion
  248.5 2.2 multiply_convert_fusion
  252.9 8.2 %all-gather.12.cloned.1.call-done = bf16[256,2048]{1,0:T(8,128)(2,1)} async-done(((bf16[128,2048]{1,0:T(8,128)(2,1)}), bf16[256,2048]{1,0:T(8,128)(2,1)}) %all-gather.12.cloned.1.call-update) | async-done | bytes 1048592 | tf_op jit(solution)/shard_map/all_gather | solution.py:123
  261.2 116.1 %all-gather.14.cloned.1.call-done = bf16[2048,2048]{1,0:T(8,128)(2,1)} async-done(((bf16[128,2048]{1,0:T(8,128)(2,1)}), bf16[2048,2048]{1,0:T(8,128)(2,1)}) %all-gather.14.cloned.1.call-update) | async-done | bytes 8388624 | tf_op jit(solution)/shard_map/all_gather | solution.py:37
  377.3 7.4 %fusion.21 = f32[256,2048]{1,0:T(8,128)} fusion(bf16[256,2048]{1,0:T(8,128)(2,1)} %all-gather.12.cloned.1.call-done, bf16[2048,2048]{1,0:T(8,128)(2,1)} %all-gather.14.cloned.1.call-done), kind=kOutput, calls=%fused_computation.39 | convolution fusion | flops 2147483648 | bytes 11534336 | tf_op jit(solution)/shard_map/dot_general | solution.py:125
  384.7 105.7 %all-gather.16.cloned.1.call-done = bf16[2048,2048]{1,0:T(8,128)(2,1)} async-done(((bf16[128,2048]{1,0:T(8,128)(2,1)}), bf16[2048,2048]{1,0:T(8,128)(2,1)}) %all-gather.16.cloned.1.call-update) | async-done | bytes 8388624 | tf_op jit(solution)/shard_map/all_gather | solution.py:38
  490.4 142.7 %all-gather.18.cloned.1.call-done = bf16[2048,2048]{1,0:T(8,128)(2,1)} async-done(((bf16[2048,128]{1,0:T(8,128)(2,1)}), bf16[2048,2048]{1,0:T(8,128)(2,1)}) %all-gather.18.cloned.1.call-update) | async-done | bytes 8388624 | tf_op jit(solution)/shard_map/all_gather | solution.py:39
  633.1 12.1 %convolution_convert_fusion.1 = bf16[256,2048]{1,0:T(8,128)(2,1)} fusion(bf16[2048,2048]{1,0:T(8,128)(2,1)} %all-gather.18.cloned.1.call-done, bf16[256,2048]{1,0:T(8,128)(2,1)S(1)} %copy-done.4, bf16[2048,2048]{1,0:T(8,128)(2,1)} %all-gather.16.cloned.1.call-done, f32[256,2048]{1,0:T(8,128)} %fusion.21), kind=kOutput, calls=%fused_computation.25 | convolution fusion | flops 4298637312 | bytes 20971520 | tf_op jit(solution)/shard_map/dot_general | solution.py:130
  645.3 6.7 %reduce-scatter.5.cloned.1.call-done = bf16[128,2048]{1,0:T(8,128)(2,1)} async-done(((bf16[256,2048]{1,0:T(8,128)(2,1)}), bf16[128,2048]{1,0:T(8,128)(2,1)}) %reduce-scatter.5.cloned.1.call-update) | async-done | bytes 524304 | tf_op jit(solution)/shard_map/reduce_scatter | solution.py:129
  652.0 2.2 add_convert_fusion
  (60 shorter events, 10.1 us)
Async XLA Ops:
  6.5 93.2 %all-gather.10.cloned.1.call-start = ((), (), s32[]{:S(2)}) async-start(), calls=%async_computation.3 | async-start | bytes 4456448 | tf_op jit(solution)/shard_map/all_gather | solution.py:92
  8.4 179.0 %all-gather.8.cloned.1.call-start = ((), (), s32[]{:S(2)}) async-start(), calls=%async_computation.2 | async-start | bytes 4456448 | tf_op jit(solution)/shard_map/all_gather | solution.py:91
  10.2 235.6 %reduce-scatter.3.cloned.1.call-start = ((), (), s32[]{:S(2)}) async-start(), calls=%async_computation.4 | async-start | bytes 1572864 | tf_op jit(solution)/shard_map/reduce_scatter | solution.py:113
  208.0 39.0 %copy-start.1 = (bf16[128,2048]{1,0:T(8,128)(2,1)S(1)}, bf16[128,2048]{1,0:T(8,128)(2,1)}, u32[]{:S(2)}) copy-start(bf16[128,2048]{1,0:T(8,128)(2,1)} %param.16) | copy-start | bytes 1572868
  208.0 39.0 %copy-start.2 = (f32[2048]{0:T(1024)S(1)}, f32[2048]{0:T(1024)}, u32[]{:S(2)}) copy-start(f32[2048]{0:T(1024)} %param.23) | copy-start | bytes 24580
  208.1 40.5 %copy-start.3 = (f32[2048]{0:T(1024)S(1)}, f32[2048]{0:T(1024)}, u32[]{:S(2)}) copy-start(f32[2048]{0:T(1024)} %param.24) | copy-start | bytes 24580
  213.0 48.2 %all-gather.12.cloned.1.call-start = ((), (), s32[]{:S(2)}) async-start(), calls=%async_computation.5 | async-start | bytes 1572864 | tf_op jit(solution)/shard_map/all_gather | solution.py:123
  250.8 126.5 %all-gather.14.cloned.1.call-start = ((), (), s32[]{:S(2)}) async-start(), calls=%async_computation.6 | async-start | bytes 8912896 | tf_op jit(solution)/shard_map/all_gather | solution.py:37
  251.4 239.1 %all-gather.16.cloned.1.call-start = ((), (), s32[]{:S(2)}) async-start(), calls=%async_computation.7 | async-start | bytes 8912896 | tf_op jit(solution)/shard_map/all_gather | solution.py:38
  251.9 381.2 %all-gather.18.cloned.1.call-start = ((), (), s32[]{:S(2)}) async-start(), calls=%async_computation.8 | async-start | bytes 8912896 | tf_op jit(solution)/shard_map/all_gather | solution.py:39
  252.7 399.4 %reduce-scatter.5.cloned.1.call-start = ((), (), s32[]{:S(2)}) async-start(), calls=%async_computation.9 | async-start | bytes 1572864 | tf_op jit(solution)/shard_map/reduce_scatter | solution.py:129
  261.2 372.0 %copy-start.4 = (bf16[256,2048]{1,0:T(8,128)(2,1)S(1)}, bf16[256,2048]{1,0:T(8,128)(2,1)}, u32[]{:S(2)}) copy-start(bf16[256,2048]{1,0:T(8,128)(2,1)} %all-gather.12.cloned.1.call-done) | copy-start | bytes 3145732
  384.7 267.3 %copy-start = (bf16[128,2048]{1,0:T(8,128)(2,1)S(1)}, bf16[128,2048]{1,0:T(8,128)(2,1)}, u32[]{:S(2)}) copy-start(bf16[128,2048]{1,0:T(8,128)(2,1)} %reduce-scatter.3.cloned.1.call-done) | copy-start | bytes 1572868
Sparse Core Ops, SparseCore 0:
  10.1 89.5 all-gather.9
  102.4 84.9 all-gather.7
  213.1 32.6 reduce-scatter.2
  250.9 10.2 all-gather.11
  263.8 113.4 all-gather.13
  379.9 110.4 all-gather.15
  493.1 139.9 all-gather.17
  645.4 6.5 reduce-scatter.4
where the time goes:
time: 662 us; the launch traced here: 661 us
  waiting for transfers between devices  545 us (82%)
  blocking collectives  43 us (6%)
  matrix products  31.2 us (5%)
  between operations  13.6 us (2%)
  local copies, waits for them, and re-layouts  11.9 us (2%)
  other arithmetic  11.2 us (2%)
    all_gather x1, waiting for transfers between devices, local(): lax.all_gather(down_weight, 'sp', axis=1, tiled=True)  143 us
    all_gather x1, waiting for transfers between devices, local(): lax.all_gather(gate_weight, 'sp', axis=0, tiled=True)  116 us
    all_gather x1, waiting for transfers between devices, local(): lax.all_gather(up_weight, 'sp', axis=0, tiled=True)  106 us
    all_gather x1, waiting for transfers between devices, local(): key_rows = lax.all_gather(keys, 'sp', axis=0, tiled=True)  87.7 us
    all_gather x1, blocking collectives, local(): doc_rows = lax.all_gather(documents, 'sp', axis=0, tiled=True)  43 us
    all_gather x1, waiting for transfers between devices, local(): value_rows = lax.all_gather(values, 'sp', axis=0, tiled=True)  42.7 us
    reduce_scatter x1, waiting for transfers between devices, local(): lax.psum_scatter(jnp.dot(rows_slice, out_weight, preferred_element_type=j...  32.8 us
  transfers between devices with their start and end apart: 8, of which 8 were waited for; matrix products, arithmetic and copies ran while one was open for 2% of the time, Pallas kernels for 0%

commit v1 on v0

--- a/solution.py
+++ b/solution.py
@@ -36,7 +36,7 @@
     collected = (
         lax.all_gather(gate_weight, "sp", axis=0, tiled=True),
         lax.all_gather(up_weight, "sp", axis=0, tiled=True),
-        lax.all_gather(down_weight, "sp", axis=1, tiled=True),
+        jnp.concatenate(lax.all_gather(down_weight, "sp"), axis=1),
     )
     residual_rows = resid.astype(jnp.float32)
 

time: 662 us -> 629 us (0.950)
  waiting for transfers between devices: 545 us -> 500 us
  local copies, waits for them, and re-layouts: 11.9 us -> 23.7 us
    all_gather x1, waiting for transfers between devices: 143 us -> 110 us  [local(): lax.all_gather(down_weight, 'sp')]
    reshape x0 -> x1, local copies, waits for them, and re-layouts: none -> 11.8 us  [local(): jnp.concatenate(lax.all_gather(down_weight, 'sp'), axis=1)]
    all_gather x1, waiting for transfers between devices: 8.25 us -> 0.01 us  [local(): normed_all = lax.all_gather(normed, 'tp', axis=0, tiled=True)]
  transfers between devices with their start and end apart: 8 -> 8, of which waited for: 8 -> 7; matrix products, arithmetic and copies ran while one was open for 2% -> 5% of each run, Pallas kernels for 0% -> 0%
where the time goes in v1:
time: 629 us; the launch traced here: 628 us
  waiting for transfers between devices  500 us (79%)
  blocking collectives  43 us (7%)
  matrix products  31.2 us (5%)
  local copies, waits for them, and re-layouts  23.7 us (4%)
  between operations  13.6 us (2%)
  other arithmetic  11.2 us (2%)
    all_gather x1, waiting for transfers between devices, local(): lax.all_gather(gate_weight, 'sp', axis=0, tiled=True)  113 us
    all_gather x1, waiting for transfers between devices, local(): lax.all_gather(down_weight, 'sp')  110 us
    all_gather x1, waiting for transfers between devices, local(): lax.all_gather(up_weight, 'sp', axis=0, tiled=True)  106 us
    all_gather x1, waiting for transfers between devices, local(): key_rows = lax.all_gather(keys, 'sp', axis=0, tiled=True)  87.7 us
    all_gather x1, blocking collectives, local(): doc_rows = lax.all_gather(documents, 'sp', axis=0, tiled=True)  43 us
    all_gather x1, waiting for transfers between devices, local(): value_rows = lax.all_gather(values, 'sp', axis=0, tiled=True)  42.7 us
    reduce_scatter x1, waiting for transfers between devices, local(): lax.psum_scatter(jnp.dot(rows_slice, out_weight, preferred_element_type=j...  32.3 us
  transfers between devices with their start and end apart: 8, of which 7 were waited for; matrix products, arithmetic and copies ran while one was open for 5% of the time, Pallas kernels for 0%

profile of v1, /device:TPU:0, one launch (start us, length us, event | category | flops | bytes accessed | tf_op | source)
XLA Modules:
  0.0 628.1 jit_solution(7884142588246619906)
XLA Ops:
  6.5 1.8 copy.36
  8.4 1.8 copy.34
  11.3 1.2 copy.35
  14.0 43.0 %all-gather.1 = s32[16,1,256]{2,1,0:T(1,128)S(1)} all-gather(s32[1,1,256]{2,1,0:T(1,128)} %bitcast.68), channel_id=1, replica_groups=mesh['sp'=16,'tp'=2] {'sp'}, dimensions={0}, use_global_device_ids=true | all-gather | bytes 17408 | tf_op jit(solution)/shard_map/all_gather | solution.py:93
  56.9 42.7 %all-gather.11.cloned.1.call-done = bf16[4096,512]{0,1:T(8,128)(2,1)} async-done(((bf16[256,512]{0,1:T(8,128)(2,1)}), bf16[4096,512]{0,1:T(8,128)(2,1)}) %all-gather.11.cloned.1.call-update) | async-done | bytes 4194320 | tf_op jit(solution)/shard_map/all_gather | solution.py:92
  99.7 87.7 %all-gather.9.cloned.1.call-done = bf16[4096,512]{0,1:T(8,128)(2,1)} async-done(((bf16[256,512]{0,1:T(8,128)(2,1)}), bf16[4096,512]{0,1:T(8,128)(2,1)}) %all-gather.9.cloned.1.call-update) | async-done | bytes 4194320 | tf_op jit(solution)/shard_map/all_gather | solution.py:91
  187.5 20.6 %while.18 = (s32[]{:T(128)}, f32[4,2,256]{2,1,0:T(2,128)S(1)}, f32[4,2,256]{2,1,0:T(2,128)S(1)}, f32[4,2,256,128]{3,2,1,0:T(8,128)S(1)}, s32[]{:T(128)}, /*index...) while((s32[]{:T(128)}, f32[4,2,256]{2,1,0:T(2,128)S(1)}, ...), condition=%wide.region_5.6_spmd.clone, body=%wide.region_0.5_spmd.clone.sunk | while | flops 1114903808 | bytes 35472848 | solution.py:107
  189.3 13.1 %conditional.3 = ((f32[4,2,256]{2,1,0:T(2,128)S(1)}, f32[4,2,256]{2,1,0:T(2,128)S(1)}, f32[4,2,256,128]{3,2,1,0:T(8,128)S(1)})) conditional(s32[]{:T(128)} %convert_element_type.92, (f32[4,2,256]{2,1,0:T(2,128)S(1)}, f32[4,2,256]{2,1,0:T(2,128)S(1)}, f32[4,2,256,128]{3,2,1,0:T(8,128)S(1)}) %tuple.53, (s32[]{:T(128)}, s32[]{:T(128)}, ...), branch_computations={%region_1.0_spmd, %region_2.4_spmd} | conditional | flops 1114903808 | bytes 35463248 | solution.py:84
  190.4 1.7 constant_dynamic-slice_fusion
  192.2 3.0 fusion.6
  195.2 3.1 fusion.5
  198.3 4.1 fusion.10
  208.6 4.4 convolution_convert_fusion
  213.6 32.3 %reduce-scatter.3.cloned.1.call-done = bf16[128,2048]{1,0:T(8,128)(2,1)} async-done(((bf16[256,2048]{1,0:T(8,128)(2,1)}), bf16[128,2048]{1,0:T(8,128)(2,1)}) %reduce-scatter.3.cloned.1.call-update) | async-done | bytes 524304 | tf_op jit(solution)/shard_map/reduce_scatter | solution.py:113
  247.2 1.4 multiply_reduce_fusion
  248.6 2.2 multiply_convert_fusion
  252.4 109.7 %all-gather.19.cloned.1.call-done = bf16[32768,128]{1,0:T(8,128)(2,1)} async-done(((bf16[2048,128]{1,0:T(8,128)(2,1)}), bf16[32768,128]{1,0:T(8,128)(2,1)}) %all-gather.19.cloned.1.call-update) | async-done | bytes 8388624 | tf_op jit(solution)/shard_map/all_gather | solution.py:39
  362.1 11.8 %copy.39 = bf16[2048,16,128]{0,2,1:T(8,128)(2,1)} copy(bf16[2048,16,128]{2,0,1:T(8,128)(2,1)} %bitcast.57) | data formatting | bytes 16777216 | tf_op jit(solution)/shard_map/reshape | solution.py:39
  374.0 112.9 %all-gather.15.cloned.1.call-done = bf16[2048,2048]{1,0:T(8,128)(2,1)} async-done(((bf16[128,2048]{1,0:T(8,128)(2,1)}), bf16[2048,2048]{1,0:T(8,128)(2,1)}) %all-gather.15.cloned.1.call-update) | async-done | bytes 8388624 | tf_op jit(solution)/shard_map/all_gather | solution.py:37
  486.9 7.4 %fusion.21 = f32[256,2048]{1,0:T(8,128)} fusion(bf16[256,2048]{1,0:T(8,128)(2,1)} %all-gather.13.cloned.1.call-done, bf16[2048,2048]{1,0:T(8,128)(2,1)} %all-gather.15.cloned.1.call-done), kind=kOutput, calls=%fused_computation.39 | convolution fusion | flops 2147483648 | bytes 11534336 | tf_op jit(solution)/shard_map/dot_general | solution.py:125
  494.3 105.9 %all-gather.17.cloned.1.call-done = bf16[2048,2048]{1,0:T(8,128)(2,1)} async-done(((bf16[128,2048]{1,0:T(8,128)(2,1)}), bf16[2048,2048]{1,0:T(8,128)(2,1)}) %all-gather.17.cloned.1.call-update) | async-done | bytes 8388624 | tf_op jit(solution)/shard_map/all_gather | solution.py:38
  600.2 12.2 %convolution_convert_fusion.1 = bf16[256,2048]{1,0:T(8,128)(2,1)} fusion(bf16[2048,2048]{0,1:T(8,128)(2,1)} %bitcast.58, bf16[256,2048]{1,0:T(8,128)(2,1)S(1)} %copy-done.4, bf16[2048,2048]{1,0:T(8,128)(2,1)} %all-gather.17.cloned.1.call-done, f32[256,2048]{1,0:T(8,128)} %fusion.21), kind=kOutput, calls=%fused_computation.25 | convolution fusion | flops 4298637312 | bytes 20971520 | tf_op jit(solution)/shard_map/dot_general | solution.py:130
  612.4 6.7 %reduce-scatter.5.cloned.1.call-done = bf16[128,2048]{1,0:T(8,128)(2,1)} async-done(((bf16[256,2048]{1,0:T(8,128)(2,1)}), bf16[128,2048]{1,0:T(8,128)(2,1)}) %reduce-scatter.5.cloned.1.call-update) | async-done | bytes 524304 | tf_op jit(solution)/shard_map/reduce_scatter | solution.py:129
  619.1 2.2 add_convert_fusion
  (61 shorter events, 10.0 us)
Async XLA Ops:
  6.5 93.2 %all-gather.11.cloned.1.call-start = ((), (), s32[]{:S(2)}) async-start(), calls=%async_computation.3 | async-start | bytes 4456448 | tf_op jit(solution)/shard_map/all_gather | solution.py:92
  8.4 179.0 %all-gather.9.cloned.1.call-start = ((), (), s32[]{:S(2)}) async-start(), calls=%async_computation.2 | async-start | bytes 4456448 | tf_op jit(solution)/shard_map/all_gather | solution.py:91
  10.2 235.7 %reduce-scatter.3.cloned.1.call-start = ((), (), s32[]{:S(2)}) async-start(), calls=%async_computation.4 | async-start | bytes 1572864 | tf_op jit(solution)/shard_map/reduce_scatter | solution.py:113
  208.1 39.1 %copy-start.1 = (bf16[128,2048]{1,0:T(8,128)(2,1)S(1)}, bf16[128,2048]{1,0:T(8,128)(2,1)}, u32[]{:S(2)}) copy-start(bf16[128,2048]{1,0:T(8,128)(2,1)} %param.16) | copy-start | bytes 1572868
  208.1 39.1 %copy-start.2 = (f32[2048]{0:T(1024)S(1)}, f32[2048]{0:T(1024)}, u32[]{:S(2)}) copy-start(f32[2048]{0:T(1024)} %param.23) | copy-start | bytes 24580
  208.1 40.5 %copy-start.3 = (f32[2048]{0:T(1024)S(1)}, f32[2048]{0:T(1024)}, u32[]{:S(2)}) copy-start(f32[2048]{0:T(1024)} %param.24) | copy-start | bytes 24580
  213.0 149.1 %all-gather.19.cloned.1.call-start = ((), (), s32[]{:S(2)}) async-start(), calls=%async_computation.9 | async-start | bytes 8912896 | tf_op jit(solution)/shard_map/all_gather | solution.py:39
  213.6 160.4 %all-gather.13.cloned.1.call-start = ((), (), s32[]{:S(2)}) async-start(), calls=%async_computation.5 | async-start | bytes 1572864 | tf_op jit(solution)/shard_map/all_gather | solution.py:123
  250.8 236.0 %all-gather.15.cloned.1.call-start = ((), (), s32[]{:S(2)}) async-start(), calls=%async_computation.6 | async-start | bytes 8912896 | tf_op jit(solution)/shard_map/all_gather | solution.py:37
  251.4 348.7 %all-gather.17.cloned.1.call-start = ((), (), s32[]{:S(2)}) async-start(), calls=%async_computation.7 | async-start | bytes 8912896 | tf_op jit(solution)/shard_map/all_gather | solution.py:38
  252.2 366.9 %reduce-scatter.5.cloned.1.call-start = ((), (), s32[]{:S(2)}) async-start(), calls=%async_computation.8 | async-start | bytes 1572864 | tf_op jit(solution)/shard_map/reduce_scatter | solution.py:129
  374.0 226.2 %copy-start.4 = (bf16[256,2048]{1,0:T(8,128)(2,1)S(1)}, bf16[256,2048]{1,0:T(8,128)(2,1)}, u32[]{:S(2)}) copy-start(bf16[256,2048]{1,0:T(8,128)(2,1)} %all-gather.13.cloned.1.call-done) | copy-start | bytes 3145732
  600.2 18.9 %copy-start = (bf16[128,2048]{1,0:T(8,128)(2,1)S(1)}, bf16[128,2048]{1,0:T(8,128)(2,1)}, u32[]{:S(2)}) copy-start(bf16[128,2048]{1,0:T(8,128)(2,1)} %reduce-scatter.3.cloned.1.call-done) | copy-start | bytes 1572868
Sparse Core Ops, SparseCore 0:
  10.1 89.5 all-gather.10
  102.4 84.9 all-gather.8
  213.1 32.7 reduce-scatter.2
  248.6 113.5 all-gather.18
  363.5 7.1 all-gather.12
  373.4 113.4 all-gather.14
  489.6 110.4 all-gather.16
  612.5 6.5 reduce-scatter.4
